TPU v7x, 32 devices: a whole 2x2x4 slice. The times are simulated.
32 devices in a mesh: kv: 8 (over z, core), tp: 4 (over y, x).
Axes of the slice: x: 2, y: 2, z: 4, core: 2. Of those that a mesh axis runs over, the one named last changes fastest.
Arguments:
- tokens: bfloat16 [64, 4096], P(None, ('kv', 'tp')), may hold values from -3 to 3
- lengths: int32 [16], replicated, may hold values from 1 to 4, 32 in all
- states: float32 [16, 16, 128, 128], P('kv', 'tp'), may hold values from -3 to 3
- gain_pre: float32 [4096], P('kv'), may hold values from 0.1 to 1.9
- pre_gate: bfloat16 [4096, 11264], P('kv', 'tp'), may hold values from -0.09375 to 0.09375
- pre_up: bfloat16 [4096, 11264], P('kv', 'tp'), may hold values from -0.09375 to 0.09375
- pre_down: bfloat16 [11264, 4096], P('tp', 'kv'), may hold values from -1 to 1
- gain_mix: float32 [4096], P('kv'), may hold values from 0.1 to 1.9
- query_weight: bfloat16 [4096, 2048], P('kv', 'tp'), may hold values from -0.09375 to 0.09375
- forget_weight: bfloat16 [4096, 2048], P('kv', 'tp'), may hold values from -0.09375 to 0.09375
- input_weight: bfloat16 [4096, 2048], P('kv', 'tp'), may hold values from -0.09375 to 0.09375
- outgate_weight: bfloat16 [4096, 2048], P('kv', 'tp'), may hold values from -0.09375 to 0.09375
- forget_floor: float32 [2048], P('tp'), may hold values from 0 to 0.9
- head_gain: float32 [128], replicated, may hold values from 0.1 to 1.9
- mix_weight: bfloat16 [2048, 4096], P('tp', 'kv'), may hold values from -1 to 1
- gain_post: float32 [4096], P('kv'), may hold values from 0.1 to 1.9
- post_gate: bfloat16 [4096, 11264], P('kv', 'tp'), may hold values from -0.09375 to 0.09375
- post_up: bfloat16 [4096, 11264], P('kv', 'tp'), may hold values from -0.09375 to 0.09375
- post_down: bfloat16 [11264, 4096], P('tp', 'kv'), may hold values from -0.0546875 to 0.0546875
Outputs:
- out_tokens: bfloat16 [64, 4096], P(None, ('kv', 'tp'))
- new_states: float32 [16, 16, 128, 128], P('kv', 'tp')
Inputs may be any that keep to these rules, and one draw needn't show every extreme that they name: `lengths`: each of the 16 sequences has 1 to 4 new tokens, 32 in all, and at least one has exactly 4.
All inputs are finite; a program needn't handle non-finite values.
Results may differ from a plain program's by a relative error of at most 0.011.
Values may be sent and summed in bfloat16 or wider, within the bound.
A program may use at most 64 MiB of HBM per device.

v0:
```python
import jax
import jax.numpy as jnp
from jax import lax
from jax.sharding import PartitionSpec as P

D = 4096
DK = 128
W = 4
EPSILON = 1e-06


def gathered_norm(shard, gain_block):
    gathered = lax.all_gather(shard, "tp", axis=1, tiled=True)
    block_squares = jnp.sum(jnp.square(gathered.astype(jnp.float32)), axis=1)
    totals = lax.psum(block_squares, "kv")
    scale = lax.rsqrt(totals[:, None] / D + EPSILON)
    return (gathered.astype(jnp.float32) * scale * gain_block).astype(jnp.bfloat16)


def half_mixer(shard, gain_block, gate_weight, up_weight, down_weight):
    normed = gathered_norm(shard, gain_block)
    half_cols = gate_weight.shape[1]
    owned = lax.psum_scatter(
        jnp.concatenate(
            [
                jnp.dot(normed, gate_weight, preferred_element_type=jnp.float32),
                jnp.dot(normed, up_weight, preferred_element_type=jnp.float32),
            ],
            axis=1,
        ),
        "kv",
        scatter_dimension=0,
        tiled=True,
    )
    hidden = (jax.nn.silu(owned[:, :half_cols]) * owned[:, half_cols:]).astype(jnp.bfloat16)
    partial_out = jnp.dot(
        lax.all_gather(hidden, "kv", axis=0, tiled=True),
        down_weight,
        preferred_element_type=jnp.float32,
    )
    return lax.psum_scatter(partial_out, "tp", scatter_dimension=1, tiled=True)


def local(
    tokens,
    lengths,
    states,
    gain_pre,
    pre_gate,
    pre_up,
    pre_down,
    gain_mix,
    query_weight,
    forget_weight,
    input_weight,
    outgate_weight,
    forget_floor,
    head_gain,
    mix_weight,
    gain_post,
    post_gate,
    post_up,
    post_down,
):
    resid_one = (
        tokens.astype(jnp.float32) + 0.5 * half_mixer(tokens, gain_pre, pre_gate, pre_up, pre_down)
    ).astype(jnp.bfloat16)
    normed = gathered_norm(resid_one, gain_mix)
    head_cols = query_weight.shape[1]
    seq_local = states.shape[0]
    heads_local = states.shape[1]
    owned = lax.psum_scatter(
        jnp.concatenate(
            [
                jnp.dot(normed, query_weight, preferred_element_type=jnp.float32),
                jnp.dot(normed, forget_weight, preferred_element_type=jnp.float32),
                jnp.dot(normed, input_weight, preferred_element_type=jnp.float32),
                jnp.dot(normed, outgate_weight, preferred_element_type=jnp.float32),
            ],
            axis=1,
        ),
        "kv",
        scatter_dimension=0,
        tiled=True,
    )
    shape_four = (seq_local, W, heads_local, DK)
    queries = jax.nn.silu(owned[:, :head_cols]).reshape(shape_four)
    forget_raw = owned[:, head_cols : 2 * head_cols].reshape(shape_four)
    fresh_values = owned[:, 2 * head_cols : 3 * head_cols].reshape(shape_four)
    gating = owned[:, 3 * head_cols :].reshape(shape_four)
    local_lengths = lax.dynamic_slice_in_dim(lengths, lax.axis_index("kv") * seq_local, seq_local)
    live_mask = jnp.arange(W, dtype=jnp.int32)[None, :] < local_lengths[:, None]
    live_four = live_mask[:, :, None, None]
    floors = forget_floor.reshape(heads_local, DK)
    forgets = jnp.where(
        live_four, floors + (1.0 - floors) * jax.nn.sigmoid(forget_raw), jnp.float32(1.0)
    )
    write_rate = 1.0 - forgets
    carried = states
    readings = []
    for offset in range(W):
        carried = (
            forgets[:, offset, :, :, None] * carried
            + write_rate[:, offset, :, :, None] * fresh_values[:, offset, :, None, :]
        )
        readings.append(
            jnp.einsum(
                "bhk,bhkv->bhv", queries[:, offset], carried, precision=lax.Precision.HIGHEST
            )
        )
    read_out = jnp.stack(readings, axis=1)
    meansq = jnp.mean(read_out * read_out, axis=3, keepdims=True)
    head_out = (
        (
            read_out
            * lax.rsqrt(meansq + EPSILON)
            * head_gain
            * jax.nn.silu(gating)
            * live_four.astype(jnp.float32)
        )
        .astype(jnp.bfloat16)
        .reshape(seq_local * W, heads_local * DK)
    )
    mixed_part = jnp.dot(
        lax.all_gather(head_out, "kv", axis=0, tiled=True),
        mix_weight,
        preferred_element_type=jnp.float32,
    )
    mixed = lax.psum_scatter(mixed_part, "tp", scatter_dimension=1, tiled=True)
    resid_two = (resid_one.astype(jnp.float32) + mixed).astype(jnp.bfloat16)
    finished = resid_two.astype(jnp.float32) + 0.5 * half_mixer(
        resid_two, gain_post, post_gate, post_up, post_down
    )
    live_rows = (
        (jnp.arange(W, dtype=jnp.int32)[None, :] < lengths[:, None])
        .reshape(-1, 1)
        .astype(jnp.float32)
    )
    outcome = (finished * live_rows).astype(jnp.bfloat16)
    return (outcome, carried)


def solution(mesh):
    placed = (
        P(None, ("kv", "tp")),
        P(),
        P("kv", "tp", None, None),
        P("kv"),
        P("kv", "tp"),
        P("kv", "tp"),
        P("tp", "kv"),
        P("kv"),
        P("kv", "tp"),
        P("kv", "tp"),
        P("kv", "tp"),
        P("kv", "tp"),
        P("tp"),
        P(),
        P("tp", "kv"),
        P("kv"),
        P("kv", "tp"),
        P("kv", "tp"),
        P("tp", "kv"),
    )
    return jax.shard_map(
        local,
        mesh=mesh,
        in_specs=placed,
        out_specs=(P(None, ("kv", "tp")), P("kv", "tp", None, None)),
        check_vma=False,
    )
```

profile of v0, /device:TPU:0, one launch (start us, length us, event | category | flops | bytes accessed | tf_op | source)
XLA Modules:
  0.0 318.7 jit_solution(17917307360592700447)
XLA Ops:
  7.2 10.1 %all_gather.18 = bf16[64,512]{1,0:T(8,128)(2,1)S(1)} all-gather(bf16[64,128]{1,0:T(8,128)(2,1)} %param.19), channel_id=1, replica_groups=mesh['kv'=8,'tp'=4] {'tp'}, dimensions={1}, use_global_device_ids=true | all-gather | bytes 81920 | tf_op jit(solution)/shard_map/all_gather | solution.py:13
  17.5 14.9 %psum.21 = f32[64]{0:T(128)S(1)} all-reduce(f32[64]{0:T(128)S(1)} %fusion.8), channel_id=1, replica_groups=mesh['kv'=8,'tp'=4] {'kv'}, use_global_device_ids=true, to_apply=%region_1.0 | all-reduce | flops 64 | bytes 512 | tf_op jit(solution)/shard_map/psum | solution.py:15
  32.4 1.5 fusion.26
  34.8 1.2 pad_maximum_fusion
  36.1 31.3 %reduce-scatter.7.cloned.1.call-done = f32[8,5632]{1,0:T(8,128)} async-done(((f32[64,5632]{1,0:T(8,128)}), f32[8,5632]{1,0:T(8,128)}) %reduce-scatter.7.cloned.1.call-update) | async-done | bytes 180240 | tf_op jit(solution)/shard_map/reduce_scatter | solution.py:23
  67.4 1.0 fusion.19
  68.4 14.4 %all_gather.19 = bf16[64,2816]{1,0:T(8,128)(2,1)S(1)} all-gather(bf16[8,2816]{1,0:T(8,128)(2,1)S(1)} %fusion.19), channel_id=1, replica_groups=mesh['kv'=8,'tp'=4] {'kv'}, dimensions={0}, use_global_device_ids=true | all-gather | bytes 405504 | tf_op jit(solution)/shard_map/all_gather | solution.py:37
  82.7 3.1 fusion.45
  85.9 22.2 %reduce-scatter.9.cloned.1.call-done = f32[64,128]{1,0:T(8,128)} async-done(((f32[64,512]{1,0:T(8,128)}), f32[64,128]{1,0:T(8,128)}) %reduce-scatter.9.cloned.1.call-update) | async-done | bytes 32784 | tf_op jit(solution)/shard_map/reduce_scatter | solution.py:41
  108.8 8.1 %all_gather.20 = bf16[64,512]{1,0:T(8,128)(2,1)S(1)} all-gather(bf16[64,128]{1,0:T(8,128)(2,1)S(1)} %add_convert_fusion.1), channel_id=1, replica_groups=mesh['kv'=8,'tp'=4] {'tp'}, dimensions={1}, use_global_device_ids=true | all-gather | bytes 81920 | tf_op jit(solution)/shard_map/all_gather | solution.py:13
  117.1 13.9 %psum.22 = f32[64]{0:T(128)S(1)} all-reduce(f32[64]{0:T(128)S(1)} %fusion.11), channel_id=1, replica_groups=mesh['kv'=8,'tp'=4] {'kv'}, use_global_device_ids=true, to_apply=%region_5.6 | all-reduce | flops 64 | bytes 512 | tf_op jit(solution)/shard_map/psum | solution.py:15
  131.0 1.3 fusion.42
  132.3 1.3 fusion.40
  133.6 1.3 fusion.38
  134.9 1.3 fusion.36
  137.3 28.2 %reduce-scatter.11.cloned.1.call-done = f32[8,2048]{1,0:T(8,128)} async-done(((f32[64,2048]{1,0:T(8,128)}), f32[8,2048]{1,0:T(8,128)}) %reduce-scatter.11.cloned.1.call-update) | async-done | bytes 65552 | tf_op jit(solution)/shard_map/reduce_scatter | solution.py:72
  167.3 1.1 fusion.17
  168.4 1.5 fusion.1
  169.9 1.3 multiply_add_fusion
  173.5 14.0 %all_gather.21 = bf16[64,512]{1,0:T(8,128)(2,1)S(1)} all-gather(bf16[8,512]{1,0:T(8,128)(2,1)S(1)} %fusion.30), channel_id=1, replica_groups=mesh['kv'=8,'tp'=4] {'kv'}, dimensions={0}, use_global_device_ids=true | all-gather | bytes 73728 | tf_op jit(solution)/shard_map/all_gather | solution.py:125
  187.5 0.8 fusion.47
  188.4 22.4 %reduce-scatter.13.cloned.1.call-done = f32[64,128]{1,0:T(8,128)} async-done(((f32[64,512]{1,0:T(8,128)}), f32[64,128]{1,0:T(8,128)}) %reduce-scatter.13.cloned.1.call-update) | async-done | bytes 32784 | tf_op jit(solution)/shard_map/reduce_scatter | solution.py:129
  211.5 8.2 %all_gather.22 = bf16[64,512]{1,0:T(8,128)(2,1)S(1)} all-gather(bf16[64,128]{1,0:T(8,128)(2,1)S(1)} %add_convert_fusion), channel_id=1, replica_groups=mesh['kv'=8,'tp'=4] {'tp'}, dimensions={1}, use_global_device_ids=true | all-gather | bytes 81920 | tf_op jit(solution)/shard_map/all_gather | solution.py:13
  219.8 13.9 %psum.23 = f32[64]{0:T(128)S(1)} all-reduce(f32[64]{0:T(128)S(1)} %fusion.14), channel_id=1, replica_groups=mesh['kv'=8,'tp'=4] {'kv'}, use_global_device_ids=true, to_apply=%region_10.11 | all-reduce | flops 64 | bytes 512 | tf_op jit(solution)/shard_map/psum | solution.py:15
  233.7 2.6 fusion.22
  237.0 1.2 pad_maximum_fusion.1
  238.3 31.2 %reduce-scatter.15.cloned.1.call-done = f32[8,5632]{1,0:T(8,128)} async-done(((f32[64,5632]{1,0:T(8,128)}), f32[8,5632]{1,0:T(8,128)}) %reduce-scatter.15.cloned.1.call-update) | async-done | bytes 180240 | tf_op jit(solution)/shard_map/reduce_scatter | solution.py:23
  269.6 1.0 fusion.18
  270.5 14.4 %all_gather.23 = bf16[64,2816]{1,0:T(8,128)(2,1)S(1)} all-gather(bf16[8,2816]{1,0:T(8,128)(2,1)S(1)} %fusion.18), channel_id=1, replica_groups=mesh['kv'=8,'tp'=4] {'kv'}, dimensions={0}, use_global_device_ids=true | all-gather | bytes 405504 | tf_op jit(solution)/shard_map/all_gather | solution.py:37
  284.9 3.1 fusion.48
  288.1 22.2 %reduce-scatter.17.cloned.1.call-done = f32[64,128]{1,0:T(8,128)} async-done(((f32[64,512]{1,0:T(8,128)}), f32[64,128]{1,0:T(8,128)}) %reduce-scatter.17.cloned.1.call-update) | async-done | bytes 32784 | tf_op jit(solution)/shard_map/reduce_scatter | solution.py:41
  310.4 1.4 multiply_convert_fusion
  (70 shorter events, 9.2 us)
Async XLA Ops:
  7.2 25.2 %copy-start = (bf16[512,2816]{1,0:T(8,128)(2,1)S(1)}, bf16[512,2816]{1,0:T(8,128)(2,1)}, u32[]{:S(2)}) copy-start(bf16[512,2816]{1,0:T(8,128)(2,1)} %param.23) | copy-start | bytes 8650756
  7.2 26.7 %copy-start.8 = (f32[512]{0:T(512)S(1)}, f32[512]{0:T(512)}, u32[]{:S(2)}) copy-start(f32[512]{0:T(512)} %param.22) | copy-start | bytes 6148
  7.2 60.2 %reduce-scatter.7.cloned.1.call-start = ((), (), s32[]{:S(2)}) async-start(), calls=%async_computation.6 | async-start | bytes 1622016 | tf_op jit(solution)/shard_map/reduce_scatter | solution.py:23
  32.3 1.8 copy-start.1
  36.1 72.0 %copy-start.6 = (bf16[64,128]{1,0:T(8,128)(2,1)S(1)}, bf16[64,128]{1,0:T(8,128)(2,1)}, u32[]{:S(2)}) copy-start(bf16[64,128]{1,0:T(8,128)(2,1)} %param.19) | copy-start | bytes 49156
  36.1 94.9 %copy-start.7 = (f32[512]{0:T(512)S(1)}, f32[512]{0:T(512)}, u32[]{:S(2)}) copy-start(f32[512]{0:T(512)} %param.26) | copy-start | bytes 6148
  36.1 72.0 %reduce-scatter.9.cloned.1.call-start = ((), (), s32[]{:S(2)}) async-start(), calls=%async_computation.7 | async-start | bytes 163840 | tf_op jit(solution)/shard_map/reduce_scatter | solution.py:41
  85.8 51.2 %copy-start.12 = (s32[16]{0:T(128)S(1)}, s32[16]{0:T(128)}, u32[]{:S(2)}) copy-start(s32[16]{0:T(128)} %param.20) | copy-start | bytes 196
  85.8 51.5 %copy-start.11 = (f32[128]{0:T(128)S(1)}, f32[128]{0:T(128)}, u32[]{:S(2)}) copy-start(f32[128]{0:T(128)} %param.32) | copy-start | bytes 1540
  85.8 51.5 %copy-start.10 = (f32[512]{0:T(512)S(1)}, f32[512]{0:T(512)}, u32[]{:S(2)}) copy-start(f32[512]{0:T(512)} %param.31) | copy-start | bytes 6148
  85.8 80.7 %copy-start.3 = (f32[2,4,128,128]{3,2,1,0:T(8,128)S(1)}, f32[2,4,128,128]{3,2,1,0:T(8,128)}, u32[]{:S(2)}) copy-start(f32[2,4,128,128]{3,2,1,0:T(8,128)} %param.21) | copy-start | bytes 1572868
  85.9 79.7 %reduce-scatter.11.cloned.1.call-start = ((), (), s32[]{:S(2)}) async-start(), calls=%async_computation.8 | async-start | bytes 589824 | tf_op jit(solution)/shard_map/reduce_scatter | solution.py:72
  137.0 73.8 %reduce-scatter.13.cloned.1.call-start = ((), (), s32[]{:S(2)}) async-start(), calls=%async_computation.9 | async-start | bytes 163840 | tf_op jit(solution)/shard_map/reduce_scatter | solution.py:129
  166.4 21.1 %copy-start.5 = (bf16[512,512]{1,0:T(8,128)(2,1)S(1)}, bf16[512,512]{1,0:T(8,128)(2,1)}, u32[]{:S(2)}) copy-start(bf16[512,512]{1,0:T(8,128)(2,1)} %param.33) | copy-start | bytes 1572868
  166.5 67.2 %copy-start.9 = (f32[512]{0:T(512)S(1)}, f32[512]{0:T(512)}, u32[]{:S(2)}) copy-start(f32[512]{0:T(512)} %param.34) | copy-start | bytes 6148
  171.2 0.8 copy-start.4
  188.3 81.2 %reduce-scatter.15.cloned.1.call-start = ((), (), s32[]{:S(2)}) async-start(), calls=%async_computation.10 | async-start | bytes 1622016 | tf_op jit(solution)/shard_map/reduce_scatter | solution.py:23
  233.7 2.7 copy-start.2
  238.3 72.1 %reduce-scatter.17.cloned.1.call-start = ((), (), s32[]{:S(2)}) async-start(), calls=%async_computation.11 | async-start | bytes 163840 | tf_op jit(solution)/shard_map/reduce_scatter | solution.py:41
Sparse Core Ops, SparseCore 0:
  36.2 31.1 reduce-scatter.6
  86.0 22.0 reduce-scatter.8
  137.1 28.3 reduce-scatter.10
  188.4 22.2 reduce-scatter.12
  238.4 31.1 reduce-scatter.14
  288.1 22.2 reduce-scatter.16
where the time goes:
time: 320 us; the launch traced here: 319 us
  waiting for transfers between devices  158 us (49%)
  blocking collectives  112 us (35%)
  matrix products  21.5 us (7%)
  between operations  14.3 us (4%)
  other arithmetic  11.7 us (4%)
    reduce_scatter x2, waiting for transfers between devices, half_mixer(): lax.psum_scatter(jnp.concatenate([jnp.dot(normed, gate_weight, preferred_...  62.5 us
    reduce_scatter x2, waiting for transfers between devices, half_mixer(): return lax.psum_scatter(partial_out, 'tp', scatter_dimension=1, tiled=True)  44.4 us
    psum x3, blocking collectives, gathered_norm(): totals = lax.psum(block_squares, 'kv')  42.6 us
    all_gather x2, blocking collectives, half_mixer(): lax.all_gather(hidden, 'kv', axis=0, tiled=True)  28.7 us
    reduce_scatter x1, waiting for transfers between devices, local(): lax.psum_scatter(jnp.concatenate([jnp.dot(normed, query_weight, preferred...  28.2 us
    all_gather x3, blocking collectives, gathered_norm(): gathered = lax.all_gather(shard, 'tp', axis=1, tiled=True)  26.4 us
    reduce_scatter x1, waiting for transfers between devices, local(): mixed = lax.psum_scatter(mixed_part, 'tp', scatter_dimension=1, tiled=True)  22.4 us
    all_gather x1, blocking collectives, local(): lax.all_gather(head_out, 'kv', axis=0, tiled=True)  14 us
  transfers between devices with their start and end apart: 6, of which 6 were waited for; matrix products, arithmetic and copies ran while one was open for 0% of the time, Pallas kernels for 0%

commit v1 on v0

--- a/solution.py
+++ b/solution.py
@@ -12,7 +12,8 @@
 def gathered_norm(shard, gain_block):
     gathered = lax.all_gather(shard, "tp", axis=1, tiled=True)
     block_squares = jnp.sum(jnp.square(gathered.astype(jnp.float32)), axis=1)
-    totals = lax.psum(block_squares, "kv")
+    k_now = lax.all_gather(block_squares, axis_name="kv")
+    totals = jnp.sum(k_now, axis=0)
     scale = lax.rsqrt(totals[:, None] / D + EPSILON)
     return (gathered.astype(jnp.float32) * scale * gain_block).astype(jnp.bfloat16)
 

time: 320 us -> 323 us (level)
    psum x3 -> x0, blocking collectives: 42.6 us -> none  [gathered_norm(): totals = lax.psum(block_squares, 'kv')]
    unnamed x0 -> x3, blocking collectives: none -> 42.6 us
where the time goes in v1:
time: 323 us; the launch traced here: 322 us
  waiting for transfers between devices  158 us (49%)
  blocking collectives  112 us (35%)
  matrix products  21.5 us (7%)
  between operations  15 us (5%)
  other arithmetic  11.8 us (4%)
  local copies, waits for them, and re-layouts  3.68 us (1%)
    reduce_scatter x2, waiting for transfers between devices, half_mixer(): lax.psum_scatter(jnp.concatenate([jnp.dot(normed, gate_weight, preferred_...  62.5 us
    reduce_scatter x2, waiting for transfers between devices, half_mixer(): return lax.psum_scatter(partial_out, 'tp', scatter_dimension=1, tiled=True)  44.5 us
    unnamed x3, blocking collectives  42.6 us
    all_gather x2, blocking collectives, half_mixer(): lax.all_gather(hidden, 'kv', axis=0, tiled=True)  28.7 us
    reduce_scatter x1, waiting for transfers between devices, local(): lax.psum_scatter(jnp.concatenate([jnp.dot(normed, query_weight, preferred...  28.4 us
    all_gather x3, blocking collectives, gathered_norm(): gathered = lax.all_gather(shard, 'tp', axis=1, tiled=True)  26.4 us
    reduce_scatter x1, waiting for transfers between devices, local(): mixed = lax.psum_scatter(mixed_part, 'tp', scatter_dimension=1, tiled=True)  22.3 us
    all_gather x1, blocking collectives, local(): lax.all_gather(head_out, 'kv', axis=0, tiled=True)  14 us
  transfers between devices with their start and end apart: 6, of which 6 were waited for; matrix products, arithmetic and copies ran while one was open for 0% of the time, Pallas kernels for 0%

profile of v1, /device:TPU:0, one launch (start us, length us, event | category | flops | bytes accessed | tf_op | source)
XLA Modules:
  0.0 321.6 jit_solution(3656840878454320972)
XLA Ops:
  7.2 10.1 %all_gather.36 = bf16[64,512]{1,0:T(8,128)(2,1)S(1)} all-gather(bf16[64,128]{1,0:T(8,128)(2,1)} %param.19), channel_id=1, replica_groups=mesh['kv'=8,'tp'=4] {'tp'}, dimensions={1}, use_global_device_ids=true | all-gather | bytes 81920 | tf_op jit(solution)/shard_map/all_gather | solution.py:13
  17.5 1.2 dynamic-slice
  19.6 14.9 %all-reduce = f32[512]{0:T(512)S(1)} all-reduce(f32[512]{0:T(512)S(1)} %dynamic-update-slice), channel_id=2, replica_groups=mesh['kv'=8,'tp'=4] {'kv'}, use_global_device_ids=true, to_apply=%add | all-reduce | flops 512 | bytes 4096
  34.6 1.5 fusion.26
  37.1 1.2 pad_maximum_fusion
  38.4 31.2 %reduce-scatter.7.cloned.1.call-done = f32[8,5632]{1,0:T(8,128)} async-done(((f32[64,5632]{1,0:T(8,128)}), f32[8,5632]{1,0:T(8,128)}) %reduce-scatter.7.cloned.1.call-update) | async-done | bytes 180240 | tf_op jit(solution)/shard_map/reduce_scatter | solution.py:24
  69.6 1.0 fusion.19
  70.6 14.4 %all_gather.39 = bf16[64,2816]{1,0:T(8,128)(2,1)S(1)} all-gather(bf16[8,2816]{1,0:T(8,128)(2,1)S(1)} %fusion.19), channel_id=1, replica_groups=mesh['kv'=8,'tp'=4] {'kv'}, dimensions={0}, use_global_device_ids=true | all-gather | bytes 405504 | tf_op jit(solution)/shard_map/all_gather | solution.py:38
  85.0 3.1 fusion.45
  88.1 22.3 %reduce-scatter.9.cloned.1.call-done = f32[64,128]{1,0:T(8,128)} async-done(((f32[64,512]{1,0:T(8,128)}), f32[64,128]{1,0:T(8,128)}) %reduce-scatter.9.cloned.1.call-update) | async-done | bytes 32784 | tf_op jit(solution)/shard_map/reduce_scatter | solution.py:42
  111.1 8.1 %all_gather.40 = bf16[64,512]{1,0:T(8,128)(2,1)S(1)} all-gather(bf16[64,128]{1,0:T(8,128)(2,1)S(1)} %add_convert_fusion.1), channel_id=1, replica_groups=mesh['kv'=8,'tp'=4] {'tp'}, dimensions={1}, use_global_device_ids=true | all-gather | bytes 81920 | tf_op jit(solution)/shard_map/all_gather | solution.py:13
  119.6 13.8 %all-reduce.1 = f32[512]{0:T(512)S(1)} all-reduce(f32[512]{0:T(512)S(1)} %dynamic-update-slice.1), channel_id=3, replica_groups=mesh['kv'=8,'tp'=4] {'kv'}, use_global_device_ids=true, to_apply=%add.1 | all-reduce | flops 512 | bytes 4096
  133.6 1.3 fusion.42
  134.9 1.3 fusion.40
  136.2 1.3 fusion.38
  137.5 1.3 fusion.36
  139.9 28.4 %reduce-scatter.11.cloned.1.call-done = f32[8,2048]{1,0:T(8,128)} async-done(((f32[64,2048]{1,0:T(8,128)}), f32[8,2048]{1,0:T(8,128)}) %reduce-scatter.11.cloned.1.call-update) | async-done | bytes 65552 | tf_op jit(solution)/shard_map/reduce_scatter | solution.py:73
  170.1 1.1 fusion.17
  171.1 1.5 fusion.1
  172.6 1.3 multiply_add_fusion
  176.2 14.0 %all_gather.43 = bf16[64,512]{1,0:T(8,128)(2,1)S(1)} all-gather(bf16[8,512]{1,0:T(8,128)(2,1)S(1)} %fusion.30), channel_id=1, replica_groups=mesh['kv'=8,'tp'=4] {'kv'}, dimensions={0}, use_global_device_ids=true | all-gather | bytes 73728 | tf_op jit(solution)/shard_map/all_gather | solution.py:126
  191.1 22.3 %reduce-scatter.13.cloned.1.call-done = f32[64,128]{1,0:T(8,128)} async-done(((f32[64,512]{1,0:T(8,128)}), f32[64,128]{1,0:T(8,128)}) %reduce-scatter.13.cloned.1.call-update) | async-done | bytes 32784 | tf_op jit(solution)/shard_map/reduce_scatter | solution.py:130
  214.2 8.1 %all_gather.44 = bf16[64,512]{1,0:T(8,128)(2,1)S(1)} all-gather(bf16[64,128]{1,0:T(8,128)(2,1)S(1)} %add_convert_fusion), channel_id=1, replica_groups=mesh['kv'=8,'tp'=4] {'tp'}, dimensions={1}, use_global_device_ids=true | all-gather | bytes 81920 | tf_op jit(solution)/shard_map/all_gather | solution.py:13
  222.7 13.8 %all-reduce.2 = f32[512]{0:T(512)S(1)} all-reduce(f32[512]{0:T(512)S(1)} %dynamic-update-slice.2), channel_id=4, replica_groups=mesh['kv'=8,'tp'=4] {'kv'}, use_global_device_ids=true, to_apply=%add.2 | all-reduce | flops 512 | bytes 4096
  236.7 2.6 fusion.22
  240.0 1.2 pad_maximum_fusion.1
  241.3 31.3 %reduce-scatter.15.cloned.1.call-done = f32[8,5632]{1,0:T(8,128)} async-done(((f32[64,5632]{1,0:T(8,128)}), f32[8,5632]{1,0:T(8,128)}) %reduce-scatter.15.cloned.1.call-update) | async-done | bytes 180240 | tf_op jit(solution)/shard_map/reduce_scatter | solution.py:24
  272.6 1.0 fusion.18
  273.5 14.4 %all_gather.47 = bf16[64,2816]{1,0:T(8,128)(2,1)S(1)} all-gather(bf16[8,2816]{1,0:T(8,128)(2,1)S(1)} %fusion.18), channel_id=1, replica_groups=mesh['kv'=8,'tp'=4] {'kv'}, dimensions={0}, use_global_device_ids=true | all-gather | bytes 405504 | tf_op jit(solution)/shard_map/all_gather | solution.py:38
  287.9 3.1 fusion.48
  291.2 22.2 %reduce-scatter.17.cloned.1.call-done = f32[64,128]{1,0:T(8,128)} async-done(((f32[64,512]{1,0:T(8,128)}), f32[64,128]{1,0:T(8,128)}) %reduce-scatter.17.cloned.1.call-update) | async-done | bytes 32784 | tf_op jit(solution)/shard_map/reduce_scatter | solution.py:42
  313.4 1.4 multiply_convert_fusion
  (83 shorter events, 11.0 us)
Async XLA Ops:
  7.2 27.4 %copy-start = (bf16[512,2816]{1,0:T(8,128)(2,1)S(1)}, bf16[512,2816]{1,0:T(8,128)(2,1)}, u32[]{:S(2)}) copy-start(bf16[512,2816]{1,0:T(8,128)(2,1)} %param.23) | copy-start | bytes 8650756
  7.2 28.9 %copy-start.8 = (f32[512]{0:T(512)S(1)}, f32[512]{0:T(512)}, u32[]{:S(2)}) copy-start(f32[512]{0:T(512)} %param.22) | copy-start | bytes 6148
  7.2 62.4 %reduce-scatter.7.cloned.1.call-start = ((), (), s32[]{:S(2)}) async-start(), calls=%async_computation.6 | async-start | bytes 1622016 | tf_op jit(solution)/shard_map/reduce_scatter | solution.py:24
  34.6 1.8 copy-start.1
  38.3 72.1 %copy-start.6 = (bf16[64,128]{1,0:T(8,128)(2,1)S(1)}, bf16[64,128]{1,0:T(8,128)(2,1)}, u32[]{:S(2)}) copy-start(bf16[64,128]{1,0:T(8,128)(2,1)} %param.19) | copy-start | bytes 49156
  38.3 95.3 %copy-start.7 = (f32[512]{0:T(512)S(1)}, f32[512]{0:T(512)}, u32[]{:S(2)}) copy-start(f32[512]{0:T(512)} %param.26) | copy-start | bytes 6148
  38.3 72.0 %reduce-scatter.9.cloned.1.call-start = ((), (), s32[]{:S(2)}) async-start(), calls=%async_computation.7 | async-start | bytes 163840 | tf_op jit(solution)/shard_map/reduce_scatter | solution.py:42
  88.0 51.6 %copy-start.12 = (s32[16]{0:T(128)S(1)}, s32[16]{0:T(128)}, u32[]{:S(2)}) copy-start(s32[16]{0:T(128)} %param.20) | copy-start | bytes 196
  88.0 51.9 %copy-start.11 = (f32[128]{0:T(128)S(1)}, f32[128]{0:T(128)}, u32[]{:S(2)}) copy-start(f32[128]{0:T(128)} %param.32) | copy-start | bytes 1540
  88.0 51.9 %copy-start.10 = (f32[512]{0:T(512)S(1)}, f32[512]{0:T(512)}, u32[]{:S(2)}) copy-start(f32[512]{0:T(512)} %param.31) | copy-start | bytes 6148
  88.0 81.2 %copy-start.3 = (f32[2,4,128,128]{3,2,1,0:T(8,128)S(1)}, f32[2,4,128,128]{3,2,1,0:T(8,128)}, u32[]{:S(2)}) copy-start(f32[2,4,128,128]{3,2,1,0:T(8,128)} %param.21) | copy-start | bytes 1572868
  88.1 80.2 %reduce-scatter.11.cloned.1.call-start = ((), (), s32[]{:S(2)}) async-start(), calls=%async_computation.8 | async-start | bytes 589824 | tf_op jit(solution)/shard_map/reduce_scatter | solution.py:73
  139.6 73.8 %reduce-scatter.13.cloned.1.call-start = ((), (), s32[]{:S(2)}) async-start(), calls=%async_computation.9 | async-start | bytes 163840 | tf_op jit(solution)/shard_map/reduce_scatter | solution.py:130
  169.1 21.1 %copy-start.5 = (bf16[512,512]{1,0:T(8,128)(2,1)S(1)}, bf16[512,512]{1,0:T(8,128)(2,1)}, u32[]{:S(2)}) copy-start(bf16[512,512]{1,0:T(8,128)(2,1)} %param.33) | copy-start | bytes 1572868
  169.3 67.4 %copy-start.9 = (f32[512]{0:T(512)S(1)}, f32[512]{0:T(512)}, u32[]{:S(2)}) copy-start(f32[512]{0:T(512)} %param.34) | copy-start | bytes 6148
  173.9 0.8 copy-start.4
  191.1 81.5 %reduce-scatter.15.cloned.1.call-start = ((), (), s32[]{:S(2)}) async-start(), calls=%async_computation.10 | async-start | bytes 1622016 | tf_op jit(solution)/shard_map/reduce_scatter | solution.py:24
  236.6 2.7 copy-start.2
  241.2 72.1 %reduce-scatter.17.cloned.1.call-start = ((), (), s32[]{:S(2)}) async-start(), calls=%async_computation.11 | async-start | bytes 163840 | tf_op jit(solution)/shard_map/reduce_scatter | solution.py:42
Sparse Core Ops, SparseCore 0:
  38.4 31.1 reduce-scatter.6
  88.2 22.1 reduce-scatter.8
  139.7 28.5 reduce-scatter.10
  191.2 22.1 reduce-scatter.12
  241.3 31.1 reduce-scatter.14
  291.1 22.1 reduce-scatter.16
